TPU v7x, 32 devices: a whole 2x2x4 slice. The times are simulated.
32 devices in a mesh: sp: 8 (over z, x), tp: 4 (over y, core).
Axes of the slice: x: 2, y: 2, z: 4, core: 2. Of those that a mesh axis runs over, the one named last changes fastest.
Arguments:
- queries: bfloat16 [4096, 2048], P('sp', 'tp'), may hold values from -90 to 90, as said below
- key_rows: bfloat16 [4096, 512], P('sp', 'tp'), may hold values from -6 to 6
- value_rows: bfloat16 [4096, 512], P('sp', 'tp'), may hold values from -6 to 6
- sink_logits: float32 [16], P('tp'), may hold values from 2 to 7
- residual: bfloat16 [4096, 2048], P('sp'), may hold values from -6 to 6
- norm_gain: float32 [2048], replicated, may hold values from 0.1 to 1.9
- out_weight: bfloat16 [2048, 2048], P('tp'), may hold values from -1.5 to 1.5
- gate_weight: bfloat16 [2048, 5632], P('sp', 'tp'), may hold values from -0.125 to 0.125
- up_weight: bfloat16 [2048, 5632], P('sp', 'tp'), may hold values from -0.125 to 0.125
- down_weight: bfloat16 [5632, 2048], P('tp', 'sp'), may hold values from -0.078125 to 0.078125
Outputs:
- mixed: bfloat16 [4096, 2048], P(('sp', 'tp'))
Inputs may be any that keep to these rules, and one draw needn't show every extreme that they name: queries are mostly of order one; some rows may be much larger.
All inputs are finite; a program needn't handle non-finite values.
Results may differ from a plain program's by a relative error of at most 0.012.
Values may be sent and summed in bfloat16 or wider, within the bound.
A program may use at most 128 MiB of HBM per device.

v0:
```python
import jax
import jax.numpy as jnp
from jax import lax
from jax.sharding import PartitionSpec as P

DH = 128
WIN = 128
EPSILON = 1e-06
MASKED = -1e30


def with_halo(cells, sides, width):
    for axis, dim in sides:
        count = lax.axis_size(axis)
        ends = count - 1
        head = lax.slice_in_dim(cells, 0, width, axis=dim)
        tail = lax.slice_in_dim(cells, cells.shape[dim] - width, cells.shape[dim], axis=dim)
        cells = jnp.concatenate(
            [
                lax.ppermute(tail, axis, [(i, (i + 1) % count) for i in range(ends)]),
                cells,
                lax.ppermute(head, axis, [((i + 1) % count, i) for i in range(ends)]),
            ],
            axis=dim,
        )
    return cells


def attend_block(query_blk, key_blk, value_blk, sink_logits, query_pos, key_pos, seq_len):
    kv_heads = key_blk.shape[1] // DH
    group_size = query_blk.shape[1] // key_blk.shape[1]
    query_four = query_blk.reshape(query_blk.shape[0], kv_heads, group_size, DH)
    key_three = key_blk.reshape(key_blk.shape[0], kv_heads, DH)
    value_three = value_blk.reshape(value_blk.shape[0], kv_heads, DH)
    scores = jnp.einsum(
        "qhgd,khd->hgqk", query_four, key_three, preferred_element_type=jnp.float32
    ) * DH ** (-0.5)
    allowed = (
        (jnp.abs(key_pos[None, :] - query_pos[:, None]) <= WIN)
        & (key_pos[None, :] >= 0)
        & (key_pos[None, :] < seq_len)
    )
    scores = jnp.where(allowed[None, None], scores, MASKED)
    sink_col = sink_logits.reshape(kv_heads, group_size)[:, :, None]
    highest = jnp.maximum(jnp.max(scores, axis=-1), sink_col)
    weights_exp = jnp.exp(scores - highest[..., None])
    denominator = jnp.sum(weights_exp, axis=-1) + jnp.exp(sink_col - highest)
    probabilities = (weights_exp / denominator[..., None]).astype(jnp.bfloat16)
    heads_out = jnp.einsum(
        "hgqk,khd->qhgd", probabilities, value_three, preferred_element_type=jnp.float32
    )
    return heads_out.astype(jnp.bfloat16).reshape(query_blk.shape[0], kv_heads * group_size * DH)


def rms_scale(rows_wide, norm_gain):
    mean_square = jnp.mean(rows_wide * rows_wide, axis=-1, keepdims=True)
    return (rows_wide * lax.rsqrt(mean_square + EPSILON) * norm_gain).astype(jnp.bfloat16)


def fetch_down(down_weight):
    return lax.all_gather(down_weight, "sp", axis=1, tiled=True)


def shards(
    queries,
    key_rows,
    value_rows,
    sink_logits,
    residual,
    norm_gain,
    out_weight,
    gate_weight,
    up_weight,
    down_weight,
):
    tok_local = queries.shape[0]
    block_len = 2 * WIN
    share_rows = tok_local // lax.axis_size("tp")
    seq_len = tok_local * lax.axis_size("sp")
    device_offset = lax.axis_index("sp") * tok_local
    kv_pair = jnp.stack([key_rows, value_rows])
    kv_ext = with_halo(kv_pair, (("sp", 1),), WIN)

    def one_block(block_index):
        block_first = block_index * block_len
        query_blk = lax.dynamic_slice_in_dim(queries, block_first, block_len, 0)
        key_blk = lax.dynamic_slice_in_dim(kv_ext[0], block_first, block_len + 2 * WIN, 0)
        value_blk = lax.dynamic_slice_in_dim(kv_ext[1], block_first, block_len + 2 * WIN, 0)
        query_pos = device_offset + block_first + jnp.arange(block_len, dtype=jnp.int32)
        key_pos = (
            device_offset + block_first - WIN + jnp.arange(block_len + 2 * WIN, dtype=jnp.int32)
        )
        return attend_block(query_blk, key_blk, value_blk, sink_logits, query_pos, key_pos, seq_len)

    blocks = lax.map(one_block, jnp.arange(tok_local // block_len, dtype=jnp.int32))
    attended = blocks.reshape(tok_local, queries.shape[1])
    own_first = lax.axis_index("tp") * share_rows
    attn_full = lax.psum(
        jnp.dot(attended, out_weight, preferred_element_type=jnp.float32).astype(jnp.bfloat16), "tp"
    ).astype(jnp.float32)
    middle_all = residual.astype(jnp.float32) + attn_full
    normed_all = rms_scale(middle_all, norm_gain)
    middle_own = lax.dynamic_slice_in_dim(middle_all, own_first, share_rows, 0)
    gate_sectioned = lax.all_gather(gate_weight, "sp", axis=0, tiled=True)
    up_sectioned = lax.all_gather(up_weight, "sp", axis=0, tiled=True)
    gate_acc = jnp.dot(normed_all, gate_sectioned, preferred_element_type=jnp.float32)
    up_acc = jnp.dot(normed_all, up_sectioned, preferred_element_type=jnp.float32)
    down_whole = fetch_down(down_weight)
    hidden = (jax.nn.silu(gate_acc) * up_acc).astype(jnp.bfloat16)
    ffn_share = lax.psum_scatter(
        jnp.dot(hidden, down_whole, preferred_element_type=jnp.float32).astype(jnp.bfloat16),
        "tp",
        scatter_dimension=0,
        tiled=True,
    ).astype(jnp.float32)
    return (middle_own + ffn_share).astype(jnp.bfloat16)


def solution(mesh):
    placed = (
        P("sp", "tp"),
        P("sp", "tp"),
        P("sp", "tp"),
        P("tp"),
        P("sp", None),
        P(),
        P("tp", None),
        P("sp", "tp"),
        P("sp", "tp"),
        P("tp", "sp"),
    )
    return jax.shard_map(
        shards, mesh=mesh, in_specs=placed, out_specs=P(("sp", "tp"), None), check_vma=False
    )
```

profile of v0, /device:TPU:0, one launch (start us, length us, event | category | flops | bytes accessed | tf_op | source)
XLA Modules:
  0.0 370.6 jit_solution(8707252518556242722)
XLA Ops:
  7.4 1.0 pad_maximum_fusion.2
  8.3 4.9 %collective-permute-start = (bf16[2,128,128]{2,1,0:T(8,128)(2,1)S(1)}, bf16[2,128,128]{2,1,0:T(8,128)(2,1)S(1)}, u32[]{:S(2)}, u32[]{:S(2)}) collective-permute-start(bf16[2,128,128]{2,1,0:T(8,128)(2,1)S(1)} %get-tuple-element.124), channel_id=1, source_target_pairs={{0,4},{4,8},{8,12},{12,16},{16,20},{20,24},{24,28},{1,5},{5,9},{9,... | collective-permute-start | bytes 196616 | tf_op jit(solution)/shard_map/ppermute | solution.py:20
  13.2 1.3 collective-permute-start.1
  14.5 0.6 collective-permute-done
  15.1 4.3 %collective-permute-done.1 = bf16[2,128,128]{2,1,0:T(8,128)(2,1)S(1)} collective-permute-done((bf16[2,128,128]{2,1,0:T(8,128)(2,1)S(1)}, bf16[2,128,128]{2,1,0:T(8,128)(2,1)S(1)}, u32[]{:S(2)}, u32[]{:S(2)}) %collective-permute-start.1) | collective-permute-done | bytes 65568 | tf_op jit(solution)/shard_map/ppermute | solution.py:22
  19.4 1.0 pad_maximum_fusion
  20.4 11.1 %while.12 = (s32[]{:T(128)}, bf16[2,256,512]{2,1,0:T(8,128)(2,1)}, bf16[2,768,128]{2,1,0:T(8,128)(2,1)S(1)}, s32[2]{0:T(128)S(1)}, s32[]{:T(128)}, /*index=5*/bf...) while((s32[]{:T(128)}, bf16[2,256,512]{2,1,0:T(8,128)(2,1)}, ...), condition=%wide.region_3.4_spmd, body=%wide.region_0.3_spmd.sunk | while | flops 273420544 | bytes 14467512 | solution.py:95
  20.4 0.6 dynamic_slice.42
  21.7 0.3 fusion.36
  22.0 1.0 constant_dynamic-slice_fusion.2
  23.0 0.1 copy.25
  23.2 0.5 fusion.37
  23.7 0.1 broadcast_maximum_fusion.2
  23.7 0.3 fusion.38
  24.0 0.1 exponential_add_fusion.2
  24.1 0.5 convolution_convert_fusion.4
  24.6 0.1 copy.26
  24.8 0.4 copy-done.2
  25.2 0.8 copy-done.3
  26.0 0.6 dynamic_slice.42
  27.3 0.3 fusion.36
  27.6 1.0 constant_dynamic-slice_fusion.2
  28.5 0.1 copy.25
  28.7 0.5 fusion.37
  29.2 0.1 broadcast_maximum_fusion.2
  29.3 0.3 fusion.38
  29.6 0.1 exponential_add_fusion.2
  29.7 0.5 convolution_convert_fusion.4
  30.2 0.1 copy.26
  30.3 0.4 copy-done.2
  30.7 0.8 copy-done.3
  31.5 3.6 convolution_convert_fusion.1
  35.2 0.0 all-gather.4.cloned.1.call-start
  35.3 0.5 all-gather.4.cloned.1.call-update
  35.8 0.0 all-gather.6.cloned.1.call-start
  35.8 0.5 all-gather.6.cloned.1.call-update
  36.4 0.0 all-gather.8.cloned.1.call-start
  36.4 0.5 all-gather.8.cloned.1.call-update
  37.0 0.0 reduce-scatter.2.cloned.1.call-start
  37.0 50.9 %all-reduce.2.cloned.1.call-done = bf16[512,2048]{1,0:T(8,128)(2,1)} async-done(((bf16[512,2048]{1,0:T(8,128)(2,1)}), bf16[512,2048]{1,0:T(8,128)(2,1)}) %all-reduce.2.cloned.1.call-update) | async-done | bytes 2097168 | tf_op jit(solution)/shard_map/psum | solution.py:98
  87.9 4.9 %convert_add_fusion = (f32[512,2048]{1,0:T(8,128)}, f32[512]{0:T(512)S(1)}) fusion(bf16[512,2048]{1,0:T(8,128)(2,1)} %all-reduce.2.cloned.1.call-done, bf16[512,2048]{1,0:T(8,128)(2,1)} %param.16), kind=kLoop, calls=%fused_computation.25 | loop fusion | flops 5242368 | bytes 8390656 | tf_op jit(solution)/shard_map/add | solution.py:101
  92.8 38.4 %all-gather.4.cloned.1.call-done = bf16[2048,1408]{1,0:T(8,128)(2,1)} async-done(((bf16[256,1408]{1,0:T(8,128)(2,1)}), bf16[2048,1408]{1,0:T(8,128)(2,1)}) %all-gather.4.cloned.1.call-update) | async-done | bytes 5767184 | tf_op jit(solution)/shard_map/all_gather | solution.py:104
  131.2 9.0 %fusion.14 = f32[512,1408]{1,0:T(8,128)} fusion(bf16[2048,1408]{1,0:T(8,128)(2,1)} %all-gather.4.cloned.1.call-done, f32[2048]{0:T(1024)S(1)} %copy-done.4, f32[512]{0:T(512)S(1)} %add_rsqrt_fusion, bf16[512,2048]{1,0:T(8,128)(2,1)} %all-reduce.2.cloned.1.call-done, bf16[512,2048]{1,0:T(8,128)(2,1)} %param.16), kind=kOutput, calls=%fused_computation.36 | convolution fusion | flops 2959081472 | bytes 12855296 | tf_op jit(solution)/shard_map/dot_general | solution.py:106
  140.2 83.4 %all-gather.6.cloned.1.call-done = bf16[2048,1408]{1,0:T(8,128)(2,1)} async-done(((bf16[256,1408]{1,0:T(8,128)(2,1)}), bf16[2048,1408]{1,0:T(8,128)(2,1)}) %all-gather.6.cloned.1.call-update) | async-done | bytes 5767184 | tf_op jit(solution)/shard_map/all_gather | solution.py:105
  223.6 93.0 %all-gather.8.cloned.1.call-done = bf16[1408,2048]{1,0:T(8,128)(2,1)} async-done(((bf16[1408,256]{1,0:T(8,128)(2,1)}), bf16[1408,2048]{1,0:T(8,128)(2,1)}) %all-gather.8.cloned.1.call-update) | async-done | bytes 5767184 | tf_op jit(solution)/shard_map/all_gather | solution.py:61
  316.5 14.6 %convolution_convert_fusion.2 = bf16[512,2048]{1,0:T(8,128)(2,1)} fusion(bf16[1408,2048]{1,0:T(8,128)(2,1)} %all-gather.8.cloned.1.call-done, bf16[2048,1408]{1,0:T(8,128)(2,1)} %all-gather.6.cloned.1.call-done, f32[512,1408]{1,0:T(8,128)} %fusion.14, f32[2048]{0:T(1024)S(1)} %copy-done.4, f32[512]{0:T(512)S(1)} %add_rsqrt_fusion, ...), kind=kOutput, calls=%fused_computation.29 | convolution fusion | flops 5917245440 | bytes 20719616 | tf_op jit(solution)/shard_map/dot_general | solution.py:111
  331.2 29.5 %reduce-scatter.2.cloned.1.call-done = bf16[128,2048]{1,0:T(8,128)(2,1)} async-done(((bf16[512,2048]{1,0:T(8,128)(2,1)}), bf16[128,2048]{1,0:T(8,128)(2,1)}) %reduce-scatter.2.cloned.1.call-update) | async-done | bytes 524304 | tf_op jit(solution)/shard_map/reduce_scatter | solution.py:110
  360.7 2.3 add_convert_fusion
  (28 shorter events, 0.2 us)
Async XLA Ops:
  7.4 24.2 %copy-start = (bf16[512,2048]{1,0:T(8,128)(2,1)S(1)}, bf16[512,2048]{1,0:T(8,128)(2,1)}, u32[]{:S(2)}) copy-start(bf16[512,2048]{1,0:T(8,128)(2,1)} %param.18) | copy-start | bytes 6291460
  7.4 80.6 %all-reduce.2.cloned.1.call-start = ((), (), s32[]{:S(2)}) async-start(), calls=%async_computation.1 | async-start | bytes 4194304 | tf_op jit(solution)/shard_map/psum | solution.py:98
  8.3 6.8 %collective-permute-start = (bf16[2,128,128]{2,1,0:T(8,128)(2,1)S(1)}, bf16[2,128,128]{2,1,0:T(8,128)(2,1)S(1)}, u32[]{:S(2)}, u32[]{:S(2)}) collective-permute-start(bf16[2,128,128]{2,1,0:T(8,128)(2,1)S(1)} %get-tuple-element.124), channel_id=1, source_target_pairs={{0,4},{4,8},{8,12},{12,16},{16,20},{20,24},{24,28},{1,5},{5,9},{9,... | collective-permute-start | bytes 196616 | tf_op jit(solution)/shard_map/ppermute | solution.py:20
  13.2 6.2 %collective-permute-start.1 = (bf16[2,128,128]{2,1,0:T(8,128)(2,1)S(1)}, bf16[2,128,128]{2,1,0:T(8,128)(2,1)S(1)}, u32[]{:S(2)}, u32[]{:S(2)}) collective-permute-start(bf16[2,128,128]{2,1,0:T(8,128)(2,1)S(1)} %get-tuple-element.125), channel_id=1, source_target_pairs={{4,0},{8,4},{12,8},{16,12},{20,16},{24,20},{28,24},{5,1},{9,5},{13... | collective-permute-start | bytes 196616 | tf_op jit(solution)/shard_map/ppermute | solution.py:22
  20.4 3.2 copy-start.1
  24.1 1.0 copy-start.2
  25.2 0.8 copy-start.3
  26.0 3.2 copy-start.1
  29.7 1.0 copy-start.2
  30.7 0.8 copy-start.3
  35.2 96.0 %all-gather.4.cloned.1.call-start = ((), (), s32[]{:S(2)}) async-start(), calls=%async_computation.2 | async-start | bytes 6488064 | tf_op jit(solution)/shard_map/all_gather | solution.py:104
  35.8 187.8 %all-gather.6.cloned.1.call-start = ((), (), s32[]{:S(2)}) async-start(), calls=%async_computation.3 | async-start | bytes 6488064 | tf_op jit(solution)/shard_map/all_gather | solution.py:105
  36.4 280.2 %all-gather.8.cloned.1.call-start = ((), (), s32[]{:S(2)}) async-start(), calls=%async_computation.4 | async-start | bytes 6488064 | tf_op jit(solution)/shard_map/all_gather | solution.py:61
  37.0 94.3 %copy-start.4 = (f32[2048]{0:T(1024)S(1)}, f32[2048]{0:T(1024)}, u32[]{:S(2)}) copy-start(f32[2048]{0:T(1024)} %param.17) | copy-start | bytes 24580
  37.0 323.7 %reduce-scatter.2.cloned.1.call-start = ((), (), s32[]{:S(2)}) async-start(), calls=%async_computation.5 | async-start | bytes 2621440 | tf_op jit(solution)/shard_map/reduce_scatter | solution.py:110
Sparse Core Ops, SparseCore 0:
  35.3 52.5 all-reduce.1
  331.3 29.3 reduce-scatter.1
Sparse Core Ops, SparseCore 1:
  37.9 93.3 all-gather.3
  133.3 90.2 all-gather.5
  225.5 91.0 all-gather.7
where the time goes:
time: 371 us
  waiting for transfers between devices  302 us (81%)
  matrix products  29.2 us (8%)
  between operations  15.1 us (4%)
  other arithmetic  10.6 us (3%)
  starting transfers between devices  6.34 us (2%)
  local copies, waits for them, and re-layouts  6.13 us (2%)
    all_gather x1, waiting for transfers between devices, fetch_down(): return lax.all_gather(down_weight, 'sp', axis=1, tiled=True)  93 us
    all_gather x1, waiting for transfers between devices, shards(): up_sectioned = lax.all_gather(up_weight, 'sp', axis=0, tiled=True)  83.4 us
    psum x1, waiting for transfers between devices, shards(): lax.psum(jnp.dot(attended, out_weight, preferred_element_type=jnp.float32...  50.9 us
    all_gather x1, waiting for transfers between devices, shards(): gate_sectioned = lax.all_gather(gate_weight, 'sp', axis=0, tiled=True)  38.4 us
    reduce_scatter x1, waiting for transfers between devices, shards(): lax.psum_scatter(jnp.dot(hidden, down_whole, preferred_element_type=jnp.f...  29.5 us
    dot_general x1, matrix products, shards(): jnp.dot(hidden, down_whole, preferred_element_type=jnp.float32)  14.6 us
    dot_general x1, matrix products, shards(): jnp.dot(normed_all, gate_sectioned, preferred_element_type=jnp.float32)  8.96 us
  transfers between devices with their start and end apart: 7, of which 7 were waited for; matrix products, arithmetic and copies ran while one was open for 4% of the time, Pallas kernels for 0%

commit v1 on v0

--- a/solution.py
+++ b/solution.py
@@ -101,7 +101,13 @@
     middle_all = residual.astype(jnp.float32) + attn_full
     normed_all = rms_scale(middle_all, norm_gain)
     middle_own = lax.dynamic_slice_in_dim(middle_all, own_first, share_rows, 0)
-    gate_sectioned = lax.all_gather(gate_weight, "sp", axis=0, tiled=True)
+    count_2 = lax.axis_size("sp")
+    held, shards_2 = (gate_weight, [gate_weight])
+    for _ in range(count_2 - 1):
+        held = lax.ppermute(held, "sp", [(i_2, (i_2 + 1) % count_2) for i_2 in range(count_2)])
+        shards_2.insert(0, held)
+    line = jnp.concatenate(shards_2, axis=0)
+    gate_sectioned = jnp.roll(line, (lax.axis_index("sp") + 1) * gate_weight.shape[0], axis=0)
     up_sectioned = lax.all_gather(up_weight, "sp", axis=0, tiled=True)
     gate_acc = jnp.dot(normed_all, gate_sectioned, preferred_element_type=jnp.float32)
     up_acc = jnp.dot(normed_all, up_sectioned, preferred_element_type=jnp.float32)

time: 371 us -> 365 us (0.984)
  waiting for transfers between devices: 302 us -> 265 us
  local copies, waits for them, and re-layouts: 6.13 us -> 29.1 us
  starting transfers between devices: 6.34 us -> 13.4 us
    ppermute x0 -> x7, waiting for transfers between devices: none -> 191 us  [shards(): lax.ppermute(held, 'sp', [(i_2, (i_2 + 1) % count_2) for i_2 in range(cou...]
    all_gather x1, waiting for transfers between devices: 83.4 us -> 0.01 us  [shards(): up_sectioned = lax.all_gather(up_weight, 'sp', axis=0, tiled=True)]
    all_gather x1, waiting for transfers between devices: 93 us -> 18.7 us  [fetch_down(): return lax.all_gather(down_weight, 'sp', axis=1, tiled=True)]
    psum x1, waiting for transfers between devices: 50.9 us -> 0.01 us  [shards(): lax.psum(jnp.dot(attended, out_weight, preferred_element_type=jnp.float32...]
    all_gather x1 -> x0, waiting for transfers between devices: 38.4 us -> none  [shards(): gate_sectioned = lax.all_gather(gate_weight, 'sp', axis=0, tiled=True)]
    unnamed x4 -> x41, local copies, waits for them, and re-layouts: 0.01 us -> 22.9 us
    reduce_scatter x1, waiting for transfers between devices: 29.5 us -> 49.2 us  [shards(): lax.psum_scatter(jnp.dot(hidden, down_whole, preferred_element_type=jnp.f...]
    ppermute x0 -> x7, starting transfers between devices: none -> 7.14 us  [shards(): lax.ppermute(held, 'sp', [(i_2, (i_2 + 1) % count_2) for i_2 in range(cou...]
  transfers between devices with their start and end apart: 7 -> 13, of which waited for: 7 -> 11; matrix products, arithmetic and copies ran while one was open for 4% -> 9% of each run, Pallas kernels for 0% -> 0%
where the time goes in v1:
time: 365 us; the launch traced here: 364 us
  waiting for transfers between devices  265 us (73%)
  matrix products  29.4 us (8%)
  local copies, waits for them, and re-layouts  29.1 us (8%)
  between operations  15 us (4%)
  starting transfers between devices  13.4 us (4%)
  other arithmetic  10.8 us (3%)
    ppermute x7, waiting for transfers between devices, shards(): lax.ppermute(held, 'sp', [(i_2, (i_2 + 1) % count_2) for i_2 in range(cou...  191 us
    reduce_scatter x1, waiting for transfers between devices, shards(): lax.psum_scatter(jnp.dot(hidden, down_whole, preferred_element_type=jnp.f...  49.2 us
    unnamed x41, local copies, waits for them, and re-layouts  22.9 us
    all_gather x1, waiting for transfers between devices, fetch_down(): return lax.all_gather(down_weight, 'sp', axis=1, tiled=True)  18.7 us
    dot_general x1, matrix products, shards(): jnp.dot(hidden, down_whole, preferred_element_type=jnp.float32)  14.6 us
    dot_general x1, matrix products, shards(): jnp.dot(normed_all, up_sectioned, preferred_element_type=jnp.float32)  9.06 us
  transfers between devices with their start and end apart: 13, of which 11 were waited for; matrix products, arithmetic and copies ran while one was open for 9% of the time, Pallas kernels for 0%

profile of v1, /device:TPU:0, one launch (start us, length us, event | category | flops | bytes accessed | tf_op | source)
XLA Modules:
  0.0 364.0 jit_solution(15467626486381936391)
XLA Ops:
  7.4 1.0 pad_maximum_fusion.2
  8.3 4.9 %collective-permute-start = (bf16[2,128,128]{2,1,0:T(8,128)(2,1)S(1)}, bf16[2,128,128]{2,1,0:T(8,128)(2,1)S(1)}, u32[]{:S(2)}, u32[]{:S(2)}) collective-permute-start(bf16[2,128,128]{2,1,0:T(8,128)(2,1)S(1)} %get-tuple-element.124), channel_id=1, source_target_pairs={{0,4},{4,8},{8,12},{12,16},{16,20},{20,24},{24,28},{1,5},{5,9},{9,... | collective-permute-start | bytes 196616 | tf_op jit(solution)/shard_map/ppermute | solution.py:20
  13.2 1.3 collective-permute-start.1
  15.1 4.3 %collective-permute-done.1 = bf16[2,128,128]{2,1,0:T(8,128)(2,1)S(1)} collective-permute-done((bf16[2,128,128]{2,1,0:T(8,128)(2,1)S(1)}, bf16[2,128,128]{2,1,0:T(8,128)(2,1)S(1)}, u32[]{:S(2)}, u32[]{:S(2)}) %collective-permute-start.1) | collective-permute-done | bytes 65568 | tf_op jit(solution)/shard_map/ppermute | solution.py:22
  19.4 1.0 pad_maximum_fusion
  20.4 10.4 %while.12 = (s32[]{:T(128)}, bf16[2,256,512]{2,1,0:T(8,128)(2,1)}, bf16[2,768,128]{2,1,0:T(8,128)(2,1)S(1)}, s32[2]{0:T(128)S(1)}, s32[]{:T(128)}, /*index=5*/bf...) while((s32[]{:T(128)}, bf16[2,256,512]{2,1,0:T(8,128)(2,1)}, ...), condition=%wide.region_3.4_spmd, body=%wide.region_0.3_spmd.sunk | while | flops 273420544 | bytes 10273660 | solution.py:95
  22.1 1.0 constant_dynamic-slice_fusion.2
  24.9 0.7 constant_dynamic-update-slice_fusion.18
  27.3 1.0 constant_dynamic-slice_fusion.2
  30.0 0.7 constant_dynamic-update-slice_fusion.18
  30.8 3.8 %convolution_convert_fusion.1 = bf16[512,2048]{1,0:T(8,128)(2,1)} fusion(bf16[512,512]{1,0:T(8,128)(2,1)} %bitcast.53, bf16[512,2048]{1,0:T(8,128)(2,1)S(1)} %copy-done), kind=kOutput, calls=%fused_computation.28 | convolution fusion | flops 1074790400 | bytes 4718592 | tf_op jit(solution)/shard_map/dot_general | solution.py:99
  35.8 2.5 collective-permute-start.2
  38.3 23.0 %collective-permute-done.2 = bf16[256,1408]{1,0:T(8,128)(2,1)S(1)} collective-permute-done((bf16[256,1408]{1,0:T(8,128)(2,1)S(1)}, bf16[256,1408]{1,0:T(8,128)(2,1)S(1)}, u32[]{:S(2)}, u32[]{:S(2)}) %collective-permute-start.2) | collective-permute-done | bytes 720928 | tf_op jit(solution)/shard_map/ppermute | solution.py:107
  61.3 0.9 copy-done.2
  62.2 2.5 collective-permute-start.3
  64.7 29.3 %collective-permute-done.3 = bf16[256,1408]{1,0:T(8,128)(2,1)S(1)} collective-permute-done((bf16[256,1408]{1,0:T(8,128)(2,1)S(1)}, bf16[256,1408]{1,0:T(8,128)(2,1)S(1)}, u32[]{:S(2)}, u32[]{:S(2)}) %collective-permute-start.3) | collective-permute-done | bytes 720928 | tf_op jit(solution)/shard_map/ppermute | solution.py:107
  94.0 0.9 copy-done.4
  95.0 32.6 %collective-permute-done.4 = bf16[256,1408]{1,0:T(8,128)(2,1)S(1)} collective-permute-done((bf16[256,1408]{1,0:T(8,128)(2,1)S(1)}, bf16[256,1408]{1,0:T(8,128)(2,1)S(1)}, u32[]{:S(2)}, u32[]{:S(2)}) %collective-permute-start.4) | collective-permute-done | bytes 720928 | tf_op jit(solution)/shard_map/ppermute | solution.py:107
  127.6 0.9 copy-done.6
  128.5 35.0 %collective-permute-done.5 = bf16[256,1408]{1,0:T(8,128)(2,1)S(1)} collective-permute-done((bf16[256,1408]{1,0:T(8,128)(2,1)S(1)}, bf16[256,1408]{1,0:T(8,128)(2,1)S(1)}, u32[]{:S(2)}, u32[]{:S(2)}) %collective-permute-start.5) | collective-permute-done | bytes 720928 | tf_op jit(solution)/shard_map/ppermute | solution.py:107
  163.5 0.9 copy-done.8
  164.4 22.0 %collective-permute-done.6 = bf16[256,1408]{1,0:T(8,128)(2,1)S(1)} collective-permute-done((bf16[256,1408]{1,0:T(8,128)(2,1)S(1)}, bf16[256,1408]{1,0:T(8,128)(2,1)S(1)}, u32[]{:S(2)}, u32[]{:S(2)}) %collective-permute-start.6) | collective-permute-done | bytes 720928 | tf_op jit(solution)/shard_map/ppermute | solution.py:107
  186.4 0.9 copy-done.10
  187.3 2.1 collective-permute-start.7
  189.4 38.6 %collective-permute-done.7 = bf16[256,1408]{1,0:T(8,128)(2,1)} collective-permute-done((bf16[256,1408]{1,0:T(8,128)(2,1)S(1)}, bf16[256,1408]{1,0:T(8,128)(2,1)}, u32[]{:S(2)}, u32[]{:S(2)}) %collective-permute-start.7) | collective-permute-done | bytes 720928 | tf_op jit(solution)/shard_map/ppermute | solution.py:107
  228.0 5.0 %convert_add_fusion = (f32[512,2048]{1,0:T(8,128)}, f32[512]{0:T(512)S(1)}) fusion(bf16[512,2048]{1,0:T(8,128)(2,1)} %all-reduce.2.cloned.1.call-done, bf16[512,2048]{1,0:T(8,128)(2,1)} %param.16), kind=kLoop, calls=%fused_computation.27 | loop fusion | flops 5242368 | bytes 8390656 | tf_op jit(solution)/shard_map/add | solution.py:101
  233.0 10.3 %collective-permute-done.8 = bf16[256,1408]{1,0:T(8,128)(2,1)} collective-permute-done((bf16[256,1408]{1,0:T(8,128)(2,1)}, bf16[256,1408]{1,0:T(8,128)(2,1)}, u32[]{:S(2)}, u32[]{:S(2)}) %collective-permute-start.8) | collective-permute-done | bytes 720928 | tf_op jit(solution)/shard_map/ppermute | solution.py:107
  243.3 2.0 constant_dynamic-update-slice_fusion.16
  245.4 2.1 constant_dynamic-update-slice_fusion.15
  247.5 0.9 constant_dynamic-update-slice_fusion.14
  248.4 0.9 constant_dynamic-update-slice_fusion.13
  249.3 0.9 constant_dynamic-update-slice_fusion.12
  250.2 0.9 constant_dynamic-update-slice_fusion.11
  251.1 0.9 constant_dynamic-update-slice_fusion.10
  252.1 0.9 constant_dynamic-update-slice_fusion.9
  253.0 2.0 constant_dynamic-update-slice_fusion.8
  255.1 2.0 constant_dynamic-update-slice_fusion.7
  257.1 0.9 constant_dynamic-update-slice_fusion.6
  258.0 1.0 constant_dynamic-update-slice_fusion.5
  259.0 1.0 constant_dynamic-update-slice_fusion.4
  259.9 0.9 constant_dynamic-update-slice_fusion.3
  260.8 0.9 constant_dynamic-update-slice_fusion.2
  261.8 0.9 constant_dynamic-update-slice_fusion.1
  262.7 9.1 %fusion.21 = f32[512,1408]{1,0:T(8,128)} fusion(bf16[2048,1408]{1,0:T(8,128)(2,1)} %all-gather.3.cloned.1.call-done, f32[2048]{0:T(1024)S(1)} %copy-done.13, f32[512]{0:T(512)S(1)} %add_rsqrt_fusion, bf16[512,2048]{1,0:T(8,128)(2,1)} %all-reduce.2.cloned.1.call-done, bf16[512,2048]{1,0:T(8,128)(2,1)} %param.16), kind=kOutput, calls=%fused_computation.54 | convolution fusion | flops 2959081472 | bytes 12855296 | tf_op jit(solution)/shard_map/dot_general | solution.py:113
  271.7 18.7 %all-gather.5.cloned.1.call-done = bf16[1408,2048]{1,0:T(8,128)(2,1)} async-done(((bf16[1408,256]{1,0:T(8,128)(2,1)}), bf16[1408,2048]{1,0:T(8,128)(2,1)}) %all-gather.5.cloned.1.call-update) | async-done | bytes 5767184 | tf_op jit(solution)/shard_map/all_gather | solution.py:61
  290.4 14.6 %convolution_convert_fusion.2 = bf16[512,2048]{1,0:T(8,128)(2,1)} fusion(bf16[1408,2048]{1,0:T(8,128)(2,1)} %all-gather.5.cloned.1.call-done, f32[512,1408]{1,0:T(8,128)} %fusion.21, bf16[4096,1408]{1,0:T(8,128)(2,1)} %constant_dynamic-update-slice_fusion.1, s32[]{:T(128)S(6)} %select_n.38, f32[2048]{0:T(1024)S(1)} %copy-done.13, ...), kind=kOutput, calls=%fused_computation.29 | convolution fusion | flops 5917245440 | bytes 20719620 | tf_op jit(solution)/shard_map/dot_general | solution.py:117
  305.1 49.2 %reduce-scatter.2.cloned.1.call-done = bf16[128,2048]{1,0:T(8,128)(2,1)} async-done(((bf16[512,2048]{1,0:T(8,128)(2,1)}), bf16[128,2048]{1,0:T(8,128)(2,1)}) %reduce-scatter.2.cloned.1.call-update) | async-done | bytes 524304 | tf_op jit(solution)/shard_map/reduce_scatter | solution.py:116
  354.3 2.3 add_convert_fusion
  (69 shorter events, 7.3 us)
Async XLA Ops:
  7.4 23.4 %copy-start = (bf16[512,2048]{1,0:T(8,128)(2,1)S(1)}, bf16[512,2048]{1,0:T(8,128)(2,1)}, u32[]{:S(2)}) copy-start(bf16[512,2048]{1,0:T(8,128)(2,1)} %param.18) | copy-start | bytes 6291460
  7.4 220.6 %all-reduce.2.cloned.1.call-start = ((), (), s32[]{:S(2)}) async-start(), calls=%async_computation.1 | async-start | bytes 4194304 | tf_op jit(solution)/shard_map/psum | solution.py:98
  8.3 6.8 %collective-permute-start = (bf16[2,128,128]{2,1,0:T(8,128)(2,1)S(1)}, bf16[2,128,128]{2,1,0:T(8,128)(2,1)S(1)}, u32[]{:S(2)}, u32[]{:S(2)}) collective-permute-start(bf16[2,128,128]{2,1,0:T(8,128)(2,1)S(1)} %get-tuple-element.124), channel_id=1, source_target_pairs={{0,4},{4,8},{8,12},{12,16},{16,20},{20,24},{24,28},{1,5},{5,9},{9,... | collective-permute-start | bytes 196616 | tf_op jit(solution)/shard_map/ppermute | solution.py:20
  13.2 6.2 %collective-permute-start.1 = (bf16[2,128,128]{2,1,0:T(8,128)(2,1)S(1)}, bf16[2,128,128]{2,1,0:T(8,128)(2,1)S(1)}, u32[]{:S(2)}, u32[]{:S(2)}) collective-permute-start(bf16[2,128,128]{2,1,0:T(8,128)(2,1)S(1)} %get-tuple-element.125), channel_id=1, source_target_pairs={{4,0},{8,4},{12,8},{16,12},{20,16},{24,20},{28,24},{5,1},{9,5},{13... | collective-permute-start | bytes 196616 | tf_op jit(solution)/shard_map/ppermute | solution.py:22
  20.4 3.3 copy-start.12
  25.6 3.3 copy-start.12
  30.8 5.0 %copy-start.1 = (bf16[256,1408]{1,0:T(8,128)(2,1)S(1)}, bf16[256,1408]{1,0:T(8,128)(2,1)}, u32[]{:S(2)}) copy-start(bf16[256,1408]{1,0:T(8,128)(2,1)} %param.19) | copy-start | bytes 2162692
  34.6 228.1 %all-gather.3.cloned.1.call-start = ((), (), s32[]{:S(2)}) async-start(), calls=%async_computation.2 | async-start | bytes 6488064 | tf_op jit(solution)/shard_map/all_gather | solution.py:111
  35.2 255.3 %all-gather.5.cloned.1.call-start = ((), (), s32[]{:S(2)}) async-start(), calls=%async_computation.3 | async-start | bytes 6488064 | tf_op jit(solution)/shard_map/all_gather | solution.py:61
  35.7 318.6 %reduce-scatter.2.cloned.1.call-start = ((), (), s32[]{:S(2)}) async-start(), calls=%async_computation.4 | async-start | bytes 2621440 | tf_op jit(solution)/shard_map/reduce_scatter | solution.py:116
  35.8 25.5 %collective-permute-start.2 = (bf16[256,1408]{1,0:T(8,128)(2,1)S(1)}, bf16[256,1408]{1,0:T(8,128)(2,1)S(1)}, u32[]{:S(2)}, u32[]{:S(2)}) collective-permute-start(bf16[256,1408]{1,0:T(8,128)(2,1)S(1)} %copy-done.1), channel_id=1, source_target_pairs={{0,4},{4,8},{8,12},{12,16},{16,20},{20,24},{24,28},{28,0},{1,5},{5... | collective-permute-start | bytes 2162696 | tf_op jit(solution)/shard_map/ppermute | solution.py:107
  61.3 0.9 copy-start.2
  62.2 31.8 %collective-permute-start.3 = (bf16[256,1408]{1,0:T(8,128)(2,1)S(1)}, bf16[256,1408]{1,0:T(8,128)(2,1)S(1)}, u32[]{:S(2)}, u32[]{:S(2)}) collective-permute-start(bf16[256,1408]{1,0:T(8,128)(2,1)S(1)} %collective-permute-done.2), channel_id=1, source_target_pairs={{0,4},{4,8},{8,12},{12,16},{16,20},{20,24},{24,28},{28,0},{1,5},{5... | collective-permute-start | bytes 2162696 | tf_op jit(solution)/shard_map/ppermute | solution.py:107
  94.0 0.9 copy-start.4
  95.0 32.6 %collective-permute-start.4 = (bf16[256,1408]{1,0:T(8,128)(2,1)S(1)}, bf16[256,1408]{1,0:T(8,128)(2,1)S(1)}, u32[]{:S(2)}, u32[]{:S(2)}) collective-permute-start(bf16[256,1408]{1,0:T(8,128)(2,1)S(1)} %collective-permute-done.3), channel_id=1, source_target_pairs={{0,4},{4,8},{8,12},{12,16},{16,20},{20,24},{24,28},{28,0},{1,5},{5... | collective-permute-start | bytes 2162696 | tf_op jit(solution)/shard_map/ppermute | solution.py:107
  127.6 0.9 copy-start.6
  128.4 35.0 %collective-permute-start.5 = (bf16[256,1408]{1,0:T(8,128)(2,1)S(1)}, bf16[256,1408]{1,0:T(8,128)(2,1)S(1)}, u32[]{:S(2)}, u32[]{:S(2)}) collective-permute-start(bf16[256,1408]{1,0:T(8,128)(2,1)S(1)} %collective-permute-done.4), channel_id=1, source_target_pairs={{0,4},{4,8},{8,12},{12,16},{16,20},{20,24},{24,28},{28,0},{1,5},{5... | collective-permute-start | bytes 2162696 | tf_op jit(solution)/shard_map/ppermute | solution.py:107
  163.5 0.9 copy-start.8
  164.4 22.0 %collective-permute-start.6 = (bf16[256,1408]{1,0:T(8,128)(2,1)S(1)}, bf16[256,1408]{1,0:T(8,128)(2,1)S(1)}, u32[]{:S(2)}, u32[]{:S(2)}) collective-permute-start(bf16[256,1408]{1,0:T(8,128)(2,1)S(1)} %collective-permute-done.5), channel_id=1, source_target_pairs={{0,4},{4,8},{8,12},{12,16},{16,20},{20,24},{24,28},{28,0},{1,5},{5... | collective-permute-start | bytes 2162696 | tf_op jit(solution)/shard_map/ppermute | solution.py:107
  186.4 0.9 copy-start.10
  187.3 40.7 %collective-permute-start.7 = (bf16[256,1408]{1,0:T(8,128)(2,1)S(1)}, bf16[256,1408]{1,0:T(8,128)(2,1)}, u32[]{:S(2)}, u32[]{:S(2)}) collective-permute-start(bf16[256,1408]{1,0:T(8,128)(2,1)S(1)} %collective-permute-done.6), channel_id=1, source_target_pairs={{0,4},{4,8},{8,12},{12,16},{16,20},{20,24},{24,28},{28,0},{1,5},{5... | collective-permute-start | bytes 2162696 | tf_op jit(solution)/shard_map/ppermute | solution.py:107
  228.0 15.4 %collective-permute-start.8 = (bf16[256,1408]{1,0:T(8,128)(2,1)}, bf16[256,1408]{1,0:T(8,128)(2,1)}, u32[]{:S(2)}, u32[]{:S(2)}) collective-permute-start(bf16[256,1408]{1,0:T(8,128)(2,1)} %collective-permute-done.7), channel_id=1, source_target_pairs={{0,4},{4,8},{8,12},{12,16},{16,20},{20,24},{24,28},{28,0},{1,5},{5... | collective-permute-start | bytes 2162696 | tf_op jit(solution)/shard_map/ppermute | solution.py:107
  228.0 19.5 %copy-start.11 = (bf16[256,1408]{1,0:T(8,128)(2,1)S(1)}, bf16[256,1408]{1,0:T(8,128)(2,1)}, u32[]{:S(2)}) copy-start(bf16[256,1408]{1,0:T(8,128)(2,1)} %copy-done.10) | copy-start | bytes 2162692
  233.0 15.4 %copy-start.9 = (bf16[256,1408]{1,0:T(8,128)(2,1)S(1)}, bf16[256,1408]{1,0:T(8,128)(2,1)}, u32[]{:S(2)}) copy-start(bf16[256,1408]{1,0:T(8,128)(2,1)} %copy-done.8) | copy-start | bytes 2162692
  233.0 16.3 %copy-start.7 = (bf16[256,1408]{1,0:T(8,128)(2,1)S(1)}, bf16[256,1408]{1,0:T(8,128)(2,1)}, u32[]{:S(2)}) copy-start(bf16[256,1408]{1,0:T(8,128)(2,1)} %copy-done.6) | copy-start | bytes 2162692
  233.0 17.2 %copy-start.5 = (bf16[256,1408]{1,0:T(8,128)(2,1)S(1)}, bf16[256,1408]{1,0:T(8,128)(2,1)}, u32[]{:S(2)}) copy-start(bf16[256,1408]{1,0:T(8,128)(2,1)} %copy-done.4) | copy-start | bytes 2162692
  233.0 18.1 %copy-start.3 = (bf16[256,1408]{1,0:T(8,128)(2,1)S(1)}, bf16[256,1408]{1,0:T(8,128)(2,1)}, u32[]{:S(2)}) copy-start(bf16[256,1408]{1,0:T(8,128)(2,1)} %copy-done.2) | copy-start | bytes 2162692
  257.1 5.6 %copy-start.13 = (f32[2048]{0:T(1024)S(1)}, f32[2048]{0:T(1024)}, u32[]{:S(2)}) copy-start(f32[2048]{0:T(1024)} %param.17) | copy-start | bytes 24580
Sparse Core Ops, SparseCore 0:
  34.7 52.5 all-reduce.1
  305.2 49.0 reduce-scatter.1
Sparse Core Ops, SparseCore 1:
  37.2 132.5 all-gather.2
  171.7 118.7 all-gather.4
